TPU v7x, 32 devices: a whole 2x2x4 slice. The times are simulated.
32 devices in a mesh: sp: 8 (over z, x), tp: 4 (over y, core).
Axes of the slice: x: 2, y: 2, z: 4, core: 2. Of those that a mesh axis runs over, the one named last changes fastest.
Arguments:
- mixer_input: bfloat16 [2048, 1024], P('sp', 'tp'), may hold values from -8 to 8
- decay_shift: float32 [2048, 64], P('sp', 'tp'), may hold values from -2.3 to 0
- pole_real: float32 [64, 64], P('tp'), may hold values from -1 to 0
- pole_imaginary: float32 [64, 64], P('tp'), may hold values from 1 to 201.06176
- log_step: float32 [64], P('tp'), may hold values from -4.15 to -3
- input_map: float32 [2, 64, 64, 16], P(None, 'tp'), may hold values from -1 to 1
- readout_matrix: float32 [2, 64, 16, 64], P(None, 'tp'), may hold values from -0.5 to 0.5
- skip: float32 [1024], P('tp'), may hold values from -6 to 6
- out_proj: bfloat16 [1024, 2048], P('tp'), may hold values from -0.1875 to 0.1875
- stream: bfloat16 [2048, 2048], P(('sp', 'tp')), may hold values from -6 to 6
- norm_gain: float32 [2048], replicated, may hold values from 0.1 to 1.9
- routes: int32 [2048, 2], P(('sp', 'tp')), may hold values from 0 to 7, all different within a row; in each aligned block of 64 rows (0 to 63, 64 to 127, ...) at most 32 rows name the same one
- route_logits: float32 [2048, 2], P(('sp', 'tp')), may hold values from -7.5 to 7.5
- w_gate: bfloat16 [8, 2048, 7168], P('sp', None, 'tp'), may hold values from -0.125 to 0.125
- w_up: bfloat16 [8, 2048, 7168], P('sp', None, 'tp'), may hold values from -0.125 to 0.125
- w_down: bfloat16 [8, 7168, 2048], P('sp', 'tp'), may hold values from -0.21875 to 0.21875
Outputs:
- layer_out: bfloat16 [2048, 2048], P(('sp', 'tp'))
Inputs may be any that keep to these rules, and one draw needn't show every extreme that they name: `routes`: in the rows of one device no expert is named more than 32 times, a bound that some block reaches; the 2 experts of a token differ.
All inputs are finite; a program needn't handle non-finite values.
Results may differ from a plain program's by a relative error of at most 0.015.
Values may be sent and summed in bfloat16 or wider, within the bound.
A program may use at most 128 MiB of HBM per device.

v0:
```python
import jax
import jax.numpy as jnp
from jax import lax
from jax.sharding import PartitionSpec as P

TOP_PRECISION = lax.Precision.HIGHEST
EPS = 1e-06
SEGMENT = 16


def prefix(value, axis, join, neutral):
    count, mine = (lax.axis_size(axis), lax.axis_index(axis))
    pieces = jax.tree.map(lambda part: lax.all_gather(part, axis), value)
    running = jax.tree.map(
        lambda part, zero: jnp.full_like(part, 0) + jnp.asarray(zero, part.dtype), value, neutral
    )

    def step(position, running):
        longer = join(running, jax.tree.map(lambda part: part[position], pieces))
        return jax.tree.map(lambda new, old: jnp.where(position < mine, new, old), longer, running)

    return lax.fori_loop(0, count - 1, step, running)


def discretize(pole_real, pole_imaginary, log_step, input_map):
    step = jnp.exp(log_step)[:, None]
    magnitude = jnp.exp(pole_real * step)
    factor_real = magnitude * jnp.cos(pole_imaginary * step)
    factor_imaginary = magnitude * jnp.sin(pole_imaginary * step)
    denominator = pole_real * pole_real + pole_imaginary * pole_imaginary
    ratio_real = ((factor_real - 1.0) * pole_real + factor_imaginary * pole_imaginary) / denominator
    ratio_imaginary = (
        factor_imaginary * pole_real - (factor_real - 1.0) * pole_imaginary
    ) / denominator
    map_real = ratio_real[:, :, None] * input_map[0] - ratio_imaginary[:, :, None] * input_map[1]
    map_imaginary = (
        ratio_real[:, :, None] * input_map[1] + ratio_imaginary[:, :, None] * input_map[0]
    )
    return (factor_real, factor_imaginary, map_real, map_imaginary)


def link(earlier, later):
    a_real, a_imag_part, x_real, x_imag_part = earlier
    b_real, b_imag_part, y_real, y_imag_part = later
    return (
        b_real * a_real - b_imag_part * a_imag_part,
        b_real * a_imag_part + b_imag_part * a_real,
        b_real * x_real - b_imag_part * x_imag_part + y_real,
        b_real * x_imag_part + b_imag_part * x_real + y_imag_part,
    )


def block_states(drive_input, shift, factors):
    factor_real, factor_imaginary, map_real, map_imaginary = factors
    rows, groups = shift.shape
    states = factor_real.shape[1]
    width = groups * states
    grouped = drive_input.reshape(rows, groups, -1)
    drive_real = jnp.einsum("sgc,gpc->sgp", grouped, map_real, precision=TOP_PRECISION).reshape(
        rows, width
    )
    drive_imaginary = jnp.einsum(
        "sgc,gpc->sgp", grouped, map_imaginary, precision=TOP_PRECISION
    ).reshape(rows, width)
    scale = jnp.exp(shift)[:, :, None]
    trans_real = (scale * factor_real[None]).reshape(rows, width)
    trans_imaginary = (scale * factor_imaginary[None]).reshape(rows, width)
    segments = rows // SEGMENT

    def arrange(value):
        return jnp.swapaxes(value.reshape(segments, SEGMENT, width), 0, 1)

    def advance(carry, item):
        new = link(carry, item)
        return (new, new)

    first = jnp.ones((segments, width), jnp.float32)
    empty = jnp.zeros((segments, width), jnp.float32)
    _, inner = lax.scan(
        advance,
        (first, empty, empty, empty),
        (
            arrange(trans_real),
            arrange(trans_imaginary),
            arrange(drive_real),
            arrange(drive_imaginary),
        ),
    )
    totals = tuple((part[-1] for part in inner))
    running = lax.associative_scan(link, totals, axis=0)
    enter = tuple(
        (
            jnp.concatenate([start, part[:-1]], axis=0)
            for start, part in zip((first[:1], empty[:1], empty[:1], empty[:1]), running)
        )
    )
    enter = tuple((part for part in enter))
    joined = link(tuple((part[None] for part in enter)), inner)

    def restore(value):
        return jnp.swapaxes(value, 0, 1).reshape(rows, groups, states)

    return tuple((restore(part) for part in joined))


def read_out(hidden_state_real, hidden_state_imaginary, readout_matrix):
    return jnp.einsum(
        "ani,nyi->any", hidden_state_real, readout_matrix[0], precision=TOP_PRECISION
    ) - jnp.einsum(
        "ani,nyi->any", hidden_state_imaginary, readout_matrix[1], precision=TOP_PRECISION
    )


def slot_numbers(route_rows, experts, capacity):
    flat = route_rows.reshape(route_rows.shape[:-2] + (-1,))
    matches = (flat[..., None] == jnp.arange(experts, dtype=jnp.int32)).astype(jnp.int32)
    earlier = jnp.cumsum(matches, axis=-2) - matches
    return flat * capacity + jnp.sum(earlier * matches, axis=-1)


def dispatch_rows(slots, normed, width):
    hits = (slots[..., None] == jnp.arange(width, dtype=jnp.int32)).astype(jnp.bfloat16)
    tokens = normed.shape[-2]
    hits = hits.reshape(slots.shape[:-1] + (tokens, -1, width)).sum(axis=-2)
    return jnp.einsum(
        "...tw,...td->...wd", hits, normed, preferred_element_type=jnp.float32
    ).astype(jnp.bfloat16)


def shards(
    mixer_input,
    decay_shift,
    pole_real,
    pole_imaginary,
    log_step,
    input_map,
    readout_matrix,
    skip,
    out_proj,
    stream,
    norm_gain,
    routes,
    route_logits,
    w_gate,
    w_up,
    w_down,
):
    factors = discretize(pole_real, pole_imaginary, log_step, input_map)
    drive_input = mixer_input.astype(jnp.float32)
    rows = mixer_input.shape[0]
    groups, states = pole_real.shape
    through_real, through_imaginary, local_real, local_imaginary = block_states(
        drive_input, decay_shift, factors
    )
    ones = jnp.ones((groups, states), jnp.float32)
    zeros = jnp.zeros((groups, states), jnp.float32)
    carried = prefix(
        (through_real[-1], through_imaginary[-1], local_real[-1], local_imaginary[-1]),
        "sp",
        link,
        (ones, zeros, zeros, zeros),
    )
    enter_real, enter_imaginary = (carried[2], carried[3])
    extra_real = through_real * enter_real[None] - through_imaginary * enter_imaginary[None]
    extra_imaginary = through_real * enter_imaginary[None] + through_imaginary * enter_real[None]
    response = read_out(local_real + extra_real, local_imaginary + extra_imaginary, readout_matrix)
    response = response.reshape(rows, -1) + skip * drive_input
    activated = jax.nn.gelu(response).astype(jnp.bfloat16)
    own_rows = rows // lax.axis_size("tp")
    projected = lax.psum_scatter(
        jnp.dot(activated, out_proj, preferred_element_type=jnp.float32),
        "tp",
        scatter_dimension=0,
        tiled=True,
    )
    mixed = (stream.astype(jnp.float32) + projected).astype(jnp.bfloat16)
    mixed_wide = mixed.astype(jnp.float32)
    normed = (
        mixed_wide
        * lax.rsqrt(jnp.mean(mixed_wide * mixed_wide, axis=-1, keepdims=True) + EPS)
        * norm_gain
    ).astype(jnp.bfloat16)
    weights = jax.nn.sigmoid(
        jnp.stack(
            [route_logits[:, 0] - route_logits[:, 1], route_logits[:, 1] - route_logits[:, 0]],
            axis=1,
        )
    )
    experts = lax.axis_size("sp") * w_gate.shape[0]
    capacity = 4 * own_rows // experts
    slot_width = experts * capacity
    model = stream.shape[1]
    own_slots = slot_numbers(routes, experts, capacity)
    outgoing = dispatch_rows(own_slots, normed, slot_width)
    arrived = lax.all_to_all(
        outgoing.reshape(experts, capacity, model), "sp", split_axis=0, concat_axis=0, tiled=True
    )
    expert_rows = lax.all_gather(arrived.reshape(-1, model), "tp", axis=0, tiled=True)
    gate = jnp.dot(expert_rows, w_gate[0], preferred_element_type=jnp.float32)
    upward = jnp.dot(expert_rows, w_up[0], preferred_element_type=jnp.float32)
    hidden = (jax.nn.silu(gate) * upward).astype(jnp.bfloat16)
    summed = lax.psum_scatter(
        jnp.dot(hidden, w_down[0], preferred_element_type=jnp.float32).astype(jnp.bfloat16),
        "tp",
        scatter_dimension=0,
        tiled=True,
    )
    expert_out = summed.reshape(-1, capacity, model)
    returned_result = lax.all_to_all(
        expert_out, "sp", split_axis=0, concat_axis=0, tiled=True
    ).reshape(slot_width, model)
    picked = (
        jnp.take(returned_result, own_slots, axis=0)
        .astype(jnp.float32)
        .reshape(own_rows, -1, model)
    )
    combined = mixed_wide + jnp.sum(picked * weights[:, :, None], axis=1)
    return combined.astype(jnp.bfloat16)


def solution(mesh):
    return jax.shard_map(
        shards,
        mesh=mesh,
        in_specs=(
            P("sp", "tp"),
            P("sp", "tp"),
            P("tp", None),
            P("tp", None),
            P("tp"),
            P(None, "tp", None, None),
            P(None, "tp", None, None),
            P("tp"),
            P("tp", None),
            P(("sp", "tp"), None),
            P(),
            P(("sp", "tp"), None),
            P(("sp", "tp"), None),
            P("sp", None, "tp"),
            P("sp", None, "tp"),
            P("sp", "tp", None),
        ),
        out_specs=P(("sp", "tp"), None),
        check_vma=False,
    )
```

profile of v0, /device:TPU:0, one launch (start us, length us, event | category | flops | bytes accessed | tf_op | source)
XLA Modules:
  0.0 520.7 jit_solution(16332389892618819120)
XLA Ops:
  9.1 2.6 convolution_bitcast_fusion.1
  11.7 2.6 convolution_bitcast_fusion
  14.3 2.5 copy.89
  16.9 1.6 reshape_reshape.8
  18.4 2.5 copy.90
  21.0 1.5 reshape_reshape.9
  26.4 48.6 %while.41 = (s32[]{:T(128)}, f32[16,1024]{1,0:T(8,128)S(1)}, f32[16,1024]{1,0:T(8,128)S(1)}, f32[16,1024]{1,0:T(8,128)}, f32[16,1024]{1,0:T(8,128)}, /*index=5*/...) while((s32[]{:T(128)}, f32[16,1024]{1,0:T(8,128)S(1)}, ...), condition=%wide.region_1.2_spmd.clone, body=%wide.region_0.1_spmd.clone.sunk | while | flops 294915 | bytes 1573535 | solution.py:79
  30.0 1.7 bitcast_dynamic-update-slice_fusion.5
  33.1 1.7 bitcast_dynamic-update-slice_fusion.5
  36.2 1.7 bitcast_dynamic-update-slice_fusion.5
  39.3 1.7 bitcast_dynamic-update-slice_fusion.5
  42.4 1.7 bitcast_dynamic-update-slice_fusion.5
  45.4 1.7 bitcast_dynamic-update-slice_fusion.5
  48.5 1.7 bitcast_dynamic-update-slice_fusion.5
  51.6 1.7 bitcast_dynamic-update-slice_fusion.5
  54.7 1.7 bitcast_dynamic-update-slice_fusion.5
  57.8 1.7 bitcast_dynamic-update-slice_fusion.5
  60.9 1.7 bitcast_dynamic-update-slice_fusion.5
  64.0 1.7 bitcast_dynamic-update-slice_fusion.5
  67.1 1.7 bitcast_dynamic-update-slice_fusion.5
  70.2 1.7 bitcast_dynamic-update-slice_fusion.5
  73.3 1.7 bitcast_dynamic-update-slice_fusion.5
  135.9 3.8 add_bitcast_fusion.2
  139.6 1.6 copy.96
  141.2 1.7 reshape.142
  142.9 32.4 %all_gather.15 = f32[8,16,64]{2,1,0:T(8,128)S(1)} all-gather(f32[1,16,64]{2,1,0:T(8,128)S(1)} %slice.431), channel_id=1, replica_groups=mesh['sp'=8,'tp'=4] {'sp'}, dimensions={0}, use_global_device_ids=true | all-gather | bytes 36864 | tf_op jit(solution)/shard_map/all_gather | solution.py:13
  175.3 2.8 copy.97
  178.1 2.8 reshape.143
  181.6 30.7 %all_gather.16 = f32[8,16,64]{2,1,0:T(8,128)S(1)} all-gather(f32[1,16,64]{2,1,0:T(8,128)S(1)} %slice.432), channel_id=1, replica_groups=mesh['sp'=8,'tp'=4] {'sp'}, dimensions={0}, use_global_device_ids=true | all-gather | bytes 36864 | tf_op jit(solution)/shard_map/all_gather | solution.py:13
  212.4 2.8 copy.95
  215.1 2.8 reshape.141
  218.6 30.5 %all_gather.17 = f32[8,16,64]{2,1,0:T(8,128)S(1)} all-gather(f32[1,16,64]{2,1,0:T(8,128)S(1)} %slice.433), channel_id=1, replica_groups=mesh['sp'=8,'tp'=4] {'sp'}, dimensions={0}, use_global_device_ids=true | all-gather | bytes 36864 | tf_op jit(solution)/shard_map/all_gather | solution.py:13
  249.2 2.8 copy.98
  252.0 2.9 reshape.144
  255.5 30.5 %all_gather.18 = f32[8,16,64]{2,1,0:T(8,128)S(1)} all-gather(f32[1,16,64]{2,1,0:T(8,128)S(1)} %slice.434), channel_id=1, replica_groups=mesh['sp'=8,'tp'=4] {'sp'}, dimensions={0}, use_global_device_ids=true | all-gather | bytes 36864 | tf_op jit(solution)/shard_map/all_gather | solution.py:13
  286.3 3.5 subtract_add_fusion
  289.8 2.5 fusion.17
  292.3 2.5 fusion.21
  295.0 1.9 fusion.39
  297.9 31.1 %reduce-scatter.3.cloned.1.call-done = f32[64,2048]{1,0:T(8,128)} async-done(((f32[256,2048]{1,0:T(8,128)}), f32[64,2048]{1,0:T(8,128)}) %reduce-scatter.3.cloned.1.call-update) | async-done | bytes 524304 | tf_op jit(solution)/shard_map/reduce_scatter | solution.py:170
  330.8 31.0 %all_to_all.10 = bf16[8,32,2048]{2,1,0:T(8,128)(2,1)} all-to-all(bf16[8,32,2048]{2,1,0:T(8,128)(2,1)S(1)} %bitcast.182), channel_id=1, replica_groups=mesh['sp'=8,'tp'=4] {'sp'}, dimensions={0} | all-to-all | bytes 2097152 | tf_op jit(solution)/shard_map/all_to_all | solution.py:195
  362.1 32.4 %all-gather.2.cloned.1.call-done = bf16[1024,2048]{1,0:T(8,128)(2,1)} async-done(((bf16[256,2048]{1,0:T(8,128)(2,1)}), bf16[1024,2048]{1,0:T(8,128)(2,1)}) %all-gather.2.cloned.1.call-update) | async-done | bytes 4194320 | tf_op jit(solution)/shard_map/all_gather | solution.py:198
  394.5 13.5 %fusion.10 = f32[1024,1792]{1,0:T(8,128)} fusion(bf16[1024,2048]{1,0:T(8,128)(2,1)} %all-gather.2.cloned.1.call-done, bf16[1,2048,1792]{2,1,0:T(8,128)(2,1)} %param.33), kind=kOutput, calls=%fused_computation.31 | convolution fusion | flops 7516192768 | bytes 18874368 | tf_op jit(solution)/shard_map/dot_general | solution.py:199
  408.0 25.9 %fusion.14 = bf16[1024,2048]{1,0:T(8,128)(2,1)} fusion(bf16[1,1792,2048]{2,1,0:T(8,128)(2,1)} %param.35, f32[1024,1792]{1,0:T(8,128)} %fusion.10, bf16[1024,2048]{1,0:T(8,128)(2,1)} %all-gather.2.cloned.1.call-done, bf16[1,2048,1792]{2,1,0:T(8,128)(2,1)} %param.34), kind=kOutput, calls=%fused_computation.34 | convolution fusion | flops 15045492736 | bytes 30408704 | tf_op jit(solution)/shard_map/dot_general | solution.py:203
  433.9 44.7 %reduce-scatter.5.cloned.1.call-done = bf16[256,2048]{1,0:T(8,128)(2,1)} async-done(((bf16[1024,2048]{1,0:T(8,128)(2,1)}), bf16[256,2048]{1,0:T(8,128)(2,1)}) %reduce-scatter.5.cloned.1.call-update) | async-done | bytes 1048592 | tf_op jit(solution)/shard_map/reduce_scatter | solution.py:202
  478.6 5.5 %all-to-all-start.1 = ((bf16[8,32,2048]{2,1,0:T(8,128)(2,1)}), bf16[8,32,2048]{2,1,0:T(8,128)(2,1)S(1)}, u32[]{:S(2)}, u32[]{:S(2)}) async-start(bf16[8,32,2048]{2,1,0:T(8,128)(2,1)} %bitcast.187), calls=%async_computation.3 | async-start | bytes 2097152 | tf_op jit(solution)/shard_map/all_to_all | solution.py:209
  484.7 25.1 %all-to-all-done.1 = bf16[8,32,2048]{2,1,0:T(8,128)(2,1)S(1)} async-done(((bf16[8,32,2048]{2,1,0:T(8,128)(2,1)}), bf16[8,32,2048]{2,1,0:T(8,128)(2,1)S(1)}, u32[]{:S(2)}, u32[]{:S(2)}) %all-to-all-start.1) | async-done | bytes 1048608 | tf_op jit(solution)/shard_map/all_to_all | solution.py:209
  511.1 2.3 multiply_reduce_fusion
  (231 shorter events, 98.5 us)
Async XLA Ops:
  6.5 288.4 %copy-start = (bf16[256,2048]{1,0:T(8,128)(2,1)S(1)}, bf16[256,2048]{1,0:T(8,128)(2,1)}, u32[]{:S(2)}) copy-start(bf16[256,2048]{1,0:T(8,128)(2,1)} %param.28) | copy-start | bytes 3145732
  6.5 322.5 %reduce-scatter.3.cloned.1.call-start = ((), (), s32[]{:S(2)}) async-start(), calls=%async_computation.4 | async-start | bytes 2621440 | tf_op jit(solution)/shard_map/reduce_scatter | solution.py:170
  16.9 5.8 %copy-start.8 = (f32[256,16]{0,1:T(8,128)S(1)}, f32[256,16]{0,1:T(8,128)}, u32[]{:S(2)}) copy-start(f32[256,16]{0,1:T(8,128)} %param.21) | copy-start | bytes 49156
  74.9 60.9 %copy-start.2 = (f32[16,16,1024]{2,1,0:T(8,128)S(1)}, f32[16,16,1024]{2,1,0:T(8,128)}, u32[]{:S(2)}) copy-start(f32[16,16,1024]{2,1,0:T(8,128)} %get-tuple-element.216) | copy-start | bytes 3145732
  74.9 60.9 %copy-start.3 = (f32[16,16,1024]{2,1,0:T(8,128)S(1)}, f32[16,16,1024]{2,1,0:T(8,128)}, u32[]{:S(2)}) copy-start(f32[16,16,1024]{2,1,0:T(8,128)} %get-tuple-element.218) | copy-start | bytes 3145732
  89.1 13.2 %copy-start.7 = (f32[4,1024]{1,0:T(4,128)}, f32[4,1024]{1,0:T(4,128)S(1)}, u32[]{:S(2)}) copy-start(f32[4,1024]{1,0:T(4,128)S(1)} %get-tuple-element.448) | copy-start | bytes 49156
  286.3 3.5 copy-start.6
  289.8 5.2 copy-start.4
  289.8 5.2 copy-start.12
  292.3 4.6 copy-start.9
  292.3 36.8 %copy-start.5 = (bf16[64,2048]{1,0:T(8,128)(2,1)S(1)}, bf16[64,2048]{1,0:T(8,128)(2,1)}, u32[]{:S(2)}) copy-start(bf16[64,2048]{1,0:T(8,128)(2,1)} %param.29) | copy-start | bytes 786436
  294.8 35.5 %copy-start.10 = (f32[2048]{0:T(1024)S(1)}, f32[2048]{0:T(1024)}, u32[]{:S(2)}) copy-start(f32[2048]{0:T(1024)} %param.30) | copy-start | bytes 24580
  296.9 97.7 %all-gather.2.cloned.1.call-start = ((), (), s32[]{:S(2)}) async-start(), calls=%async_computation.5 | async-start | bytes 5242880 | tf_op jit(solution)/shard_map/all_gather | solution.py:198
  361.8 116.8 %reduce-scatter.5.cloned.1.call-start = ((), (), s32[]{:S(2)}) async-start(), calls=%async_computation.6 | async-start | bytes 5242880 | tf_op jit(solution)/shard_map/reduce_scatter | solution.py:202
  433.9 50.6 %copy-start.11 = (f32[64,2]{0,1:T(2,128)S(1)}, f32[64,2]{0,1:T(2,128)}, u32[]{:S(2)}) copy-start(f32[64,2]{0,1:T(2,128)} %param.32) | copy-start | bytes 1540
  478.6 31.2 %all-to-all-start.1 = ((bf16[8,32,2048]{2,1,0:T(8,128)(2,1)}), bf16[8,32,2048]{2,1,0:T(8,128)(2,1)S(1)}, u32[]{:S(2)}, u32[]{:S(2)}) async-start(bf16[8,32,2048]{2,1,0:T(8,128)(2,1)} %bitcast.187), calls=%async_computation.3 | async-start | bytes 2097152 | tf_op jit(solution)/shard_map/all_to_all | solution.py:209
  484.2 30.0 %copy-start.1 = (bf16[256,2048]{1,0:T(8,128)(2,1)S(1)}, bf16[256,2048]{1,0:T(8,128)(2,1)}, u32[]{:S(2)}) copy-start(bf16[256,2048]{1,0:T(8,128)(2,1)} %param.28) | copy-start | bytes 3145732
Sparse Core Ops, SparseCore 0:
  297.0 32.0 reduce-scatter.2
  362.0 32.5 all-gather.1
  434.0 44.5 reduce-scatter.4
where the time goes:
time: 525 us; the launch traced here: 521 us
  blocking collectives  155 us (30%)
  waiting for transfers between devices  133 us (25%)
  local copies, waits for them, and re-layouts  95.6 us (18%)
  other arithmetic  64.7 us (12%)
  matrix products  51.8 us (10%)
  between operations  13.7 us (3%)
  starting transfers between devices  5.82 us (1%)
    all_gather x4, blocking collectives, prefix(): pieces = jax.tree.map(lambda part: lax.all_gather(part, axis), value)  124 us
    reduce_scatter x1, waiting for transfers between devices, shards(): lax.psum_scatter(jnp.dot(hidden, w_down[0], preferred_element_type=jnp.fl...  44.7 us
    all_gather x1, waiting for transfers between devices, shards(): lax.all_gather(arrived.reshape(-1, model), 'tp', axis=0, tiled=True)  32.4 us
    reduce_scatter x1, waiting for transfers between devices, shards(): lax.psum_scatter(jnp.dot(activated, out_proj, preferred_element_type=jnp....  31.1 us
    all_to_all x1, blocking collectives, shards(): lax.all_to_all(outgoing.reshape(experts, capacity, model), 'sp', split_ax...  31 us
    slice x41, local copies, waits for them, and re-layouts, block_states(): running = lax.associative_scan(link, totals, axis=0)  27.4 us
    dot_general x1, matrix products, shards(): jnp.dot(hidden, w_down[0], preferred_element_type=jnp.float32)  25.9 us
    dynamic_update_slice x16, other arithmetic, block_states(): lax.scan(advance, (first, empty, empty, empty), (arrange(trans_real), arr...  25.9 us
  transfers between devices with their start and end apart: 4, of which 4 were waited for; matrix products, arithmetic and copies ran while one was open for 0% of the time, Pallas kernels for 0%

commit v1 on v0

v1 whole, which is shorter than its diff:
```python
import functools

import jax
import jax.numpy as jnp
from jax import lax
from jax.experimental import pallas as pl
from jax.experimental.pallas import tpu as pltpu
from jax.sharding import PartitionSpec as P

TOP_PRECISION = lax.Precision.HIGHEST
EPS = 1e-06
LANES = 8
MESH = pl.DeviceIdType.MESH


def discretize(pole_real, pole_imaginary, log_step, input_map):
    step = jnp.exp(log_step)[:, None]
    magnitude = jnp.exp(pole_real * step)
    factor_real = magnitude * jnp.cos(pole_imaginary * step)
    factor_imaginary = magnitude * jnp.sin(pole_imaginary * step)
    denominator = pole_real * pole_real + pole_imaginary * pole_imaginary
    ratio_real = ((factor_real - 1.0) * pole_real + factor_imaginary * pole_imaginary) / denominator
    ratio_imaginary = (
        factor_imaginary * pole_real - (factor_real - 1.0) * pole_imaginary
    ) / denominator
    map_real = ratio_real[:, :, None] * input_map[0] - ratio_imaginary[:, :, None] * input_map[1]
    map_imaginary = (
        ratio_real[:, :, None] * input_map[1] + ratio_imaginary[:, :, None] * input_map[0]
    )
    return (factor_real, factor_imaginary, map_real, map_imaginary)


def on_ring(body, axis):
    count, mine = lax.axis_size(axis), lax.axis_index(axis)
    barrier = pltpu.get_barrier_semaphore()
    for ahead in range(1, count):
        pl.semaphore_signal(
            barrier,
            inc=1,
            device_id={axis: lax.rem(mine + ahead, count)},
            device_id_type=MESH,
        )
    pl.semaphore_wait(barrier, count - 1)
    body(count, mine)


def exchange_kernel(axis, gather, value, result, send, receive, own):
    def body(count, mine):
        copies = []
        for ahead in range(1, count):
            peer = lax.rem(mine + ahead, count)
            copy = pltpu.make_async_remote_copy(
                src_ref=value if gather else value.at[peer],
                dst_ref=result.at[mine],
                send_sem=send.at[ahead],
                recv_sem=receive.at[ahead],
                device_id={axis: peer},
                device_id_type=MESH,
            )
            copy.start()
            copies.append(copy)
        kept = pltpu.make_async_copy(value if gather else value.at[mine], result.at[mine], own)
        kept.start()
        kept.wait()
        for copy in copies:
            copy.wait()

    on_ring(body, axis)


def exchange(value, axis, number, gather=False):
    count = lax.axis_size(axis)
    shape = ((count,) + value.shape) if gather else value.shape
    return pl.pallas_call(
        functools.partial(exchange_kernel, axis, gather),
        out_shape=jax.ShapeDtypeStruct(shape, value.dtype),
        in_specs=[pl.BlockSpec(memory_space=pltpu.VMEM)],
        out_specs=pl.BlockSpec(memory_space=pltpu.VMEM),
        scratch_shapes=[
            pltpu.SemaphoreType.DMA((count,)),
            pltpu.SemaphoreType.DMA((count,)),
            pltpu.SemaphoreType.DMA,
        ],
        compiler_params=pltpu.CompilerParams(collective_id=number, has_side_effects=True),
        name=f"exchange_{number}",
    )(value)


def across(left, right):
    return lax.dot_general(
        left, right, (((1,), (1,)), ((), ())), preferred_element_type=jnp.float32
    )


def prepare(values, shift, maps, scale, drive_real, drive_imaginary):
    groups, width = shift.shape[1], scale.shape[1]
    spread = lax.broadcasted_iota(jnp.int32, (groups, width), 1) // (width // groups)
    hot = (spread == lax.broadcasted_iota(jnp.int32, (groups, width), 0)).astype(jnp.float32)
    scale[...] = jnp.dot(
        jnp.exp(shift[...]), hot, precision=TOP_PRECISION, preferred_element_type=jnp.float32
    )
    entries = values[...]
    drive_real[...] = across(entries, maps[0]) + across(entries, maps[1])
    drive_imaginary[...] = across(entries, maps[2]) + across(entries, maps[3])


def totals_kernel(values, shift, factor, maps, parts, total, scale, drive_real, drive_imaginary):
    prepare(values, shift, maps, scale, drive_real, drive_imaginary)
    width = scale.shape[1]
    wide = (LANES, width)
    factor_real = jnp.broadcast_to(factor[0:1, :], wide)
    factor_imaginary = jnp.broadcast_to(factor[1:2, :], wide)

    def step(position, carry):
        a_real, a_imaginary, x_real, x_imaginary = carry
        rows = pl.ds(pl.multiple_of(position * LANES, LANES), LANES)
        grow = scale[rows, :]
        b_real, b_imaginary = grow * factor_real, grow * factor_imaginary
        return (
            b_real * a_real - b_imaginary * a_imaginary,
            b_real * a_imaginary + b_imaginary * a_real,
            b_real * x_real - b_imaginary * x_imaginary + drive_real[rows, :],
            b_real * x_imaginary + b_imaginary * x_real + drive_imaginary[rows, :],
        )

    empty = jnp.zeros(wide, jnp.float32)
    ends = lax.fori_loop(
        0, scale.shape[0] // LANES, step, (jnp.ones(wide, jnp.float32), empty, empty, empty)
    )
    for place, end in enumerate(ends):
        parts[place] = end
    run = tuple(end[0:1] for end in ends)
    for segment in range(1, LANES):
        b_real, b_imaginary, y_real, y_imaginary = (
            end[segment : segment + 1] for end in ends
        )
        a_real, a_imaginary, x_real, x_imaginary = run
        run = (
            b_real * a_real - b_imaginary * a_imaginary,
            b_real * a_imaginary + b_imaginary * a_real,
            b_real * x_real - b_imaginary * x_imaginary + y_real,
            b_real * x_imaginary + b_imaginary * x_real + y_imaginary,
        )
    total[...] = jnp.concatenate(run + (jnp.zeros((LANES - 4, width), jnp.float32),), axis=0)


def split(value):
    high = value.astype(jnp.bfloat16)
    return high, (value - high.astype(jnp.float32)).astype(jnp.bfloat16)


def respond_kernel(
    axis, values, shift, factor, maps, parts, gathered, reads, skip, out,
    scale, drive_real, drive_imaginary,
):
    prepare(values, shift, maps, scale, drive_real, drive_imaginary)
    width = scale.shape[1]
    mine = lax.axis_index(axis)

    def before(position, carry):
        real, imaginary = carry
        item = gathered[position]
        a_real, a_imaginary = item[0:1], item[1:2]
        keep = position < mine
        return (
            jnp.where(keep, a_real * real - a_imaginary * imaginary + item[2:3], real),
            jnp.where(keep, a_real * imaginary + a_imaginary * real + item[3:4], imaginary),
        )

    none = jnp.zeros((1, width), jnp.float32)
    real, imaginary = lax.fori_loop(0, gathered.shape[0] - 1, before, (none, none))
    reals, imaginaries = [real], [imaginary]
    for segment in range(LANES - 1):
        at = slice(segment, segment + 1)
        a_real, a_imaginary = parts[0, at, :], parts[1, at, :]
        real, imaginary = (
            a_real * real - a_imaginary * imaginary + parts[2, at, :],
            a_real * imaginary + a_imaginary * real + parts[3, at, :],
        )
        reals.append(real)
        imaginaries.append(imaginary)
    wide = (LANES, width)
    factor_real = jnp.broadcast_to(factor[0:1, :], wide)
    factor_imaginary = jnp.broadcast_to(factor[1:2, :], wide)

    def step(position, carry):
        x_real, x_imaginary = carry
        rows = pl.ds(pl.multiple_of(position * LANES, LANES), LANES)
        grow = scale[rows, :]
        b_real, b_imaginary = grow * factor_real, grow * factor_imaginary
        new_real = b_real * x_real - b_imaginary * x_imaginary + drive_real[rows, :]
        new_imaginary = b_real * x_imaginary + b_imaginary * x_real + drive_imaginary[rows, :]
        drive_real[rows, :] = new_real
        drive_imaginary[rows, :] = new_imaginary
        return new_real, new_imaginary

    lax.fori_loop(
        0,
        scale.shape[0] // LANES,
        step,
        (jnp.concatenate(reals, axis=0), jnp.concatenate(imaginaries, axis=0)),
    )
    high, low = split(drive_real[...])
    response = across(high, reads[0]) + across(low, reads[0]) + across(high, reads[1])
    high, low = split(drive_imaginary[...])
    response -= across(high, reads[2]) + across(low, reads[2]) + across(high, reads[3])
    response += skip[...] * values[...].astype(jnp.float32)
    out[...] = jax.nn.gelu(response).astype(jnp.bfloat16)


def diagonal(blocks):
    groups, rows, columns = blocks.shape
    tiled = jnp.tile(blocks.reshape(groups * rows, columns), (1, groups))
    row = lax.broadcasted_iota(jnp.int32, tiled.shape, 0) // rows
    column = lax.broadcasted_iota(jnp.int32, tiled.shape, 1) // columns
    return split(jnp.where(row == column, tiled, 0.0))


def mixer(mixer_input, decay_shift, factors, readout_matrix, skip):
    factor_real, factor_imaginary, map_real, map_imaginary = factors
    rows, channels = mixer_input.shape
    groups, states = factor_real.shape
    width = groups * states

    def arrange(value):
        return jnp.swapaxes(value.reshape(LANES, rows // LANES, -1), 0, 1).reshape(rows, -1)

    values, shift = arrange(mixer_input), arrange(decay_shift)
    factor = jnp.stack([factor_real.reshape(width), factor_imaginary.reshape(width)])
    maps = jnp.stack(diagonal(map_real) + diagonal(map_imaginary))
    reads = jnp.stack(
        diagonal(readout_matrix[0]) + diagonal(readout_matrix[1])
    )
    vmem = pl.BlockSpec(memory_space=pltpu.VMEM)
    scratch = [pltpu.VMEM((rows, width), jnp.float32)] * 3
    parts, total = pl.pallas_call(
        totals_kernel,
        out_shape=(
            jax.ShapeDtypeStruct((4, LANES, width), jnp.float32),
            jax.ShapeDtypeStruct((LANES, width), jnp.float32),
        ),
        in_specs=[vmem] * 4,
        out_specs=(vmem, vmem),
        scratch_shapes=scratch,
        name="totals",
    )(values, shift, factor, maps)
    gathered = exchange(total, "sp", 0, gather=True)
    activated = pl.pallas_call(
        functools.partial(respond_kernel, "sp"),
        out_shape=jax.ShapeDtypeStruct((rows, channels), jnp.bfloat16),
        in_specs=[vmem] * 8,
        out_specs=vmem,
        scratch_shapes=scratch,
        name="respond",
    )(values, shift, factor, maps, parts, gathered, reads, skip.reshape(1, -1))
    return jnp.swapaxes(activated.reshape(rows // LANES, LANES, channels), 0, 1)


def slot_numbers(route_rows, experts, capacity):
    flat = route_rows.reshape(route_rows.shape[:-2] + (-1,))
    matches = (flat[..., None] == jnp.arange(experts, dtype=jnp.int32)).astype(jnp.int32)
    earlier = jnp.cumsum(matches, axis=-2) - matches
    return flat * capacity + jnp.sum(earlier * matches, axis=-1)


def dispatch_rows(slots, normed, width):
    hits = (slots[..., None] == jnp.arange(width, dtype=jnp.int32)).astype(jnp.bfloat16)
    tokens = normed.shape[-2]
    hits = hits.reshape(slots.shape[:-1] + (tokens, -1, width)).sum(axis=-2)
    return jnp.einsum(
        "...tw,...td->...wd", hits, normed, preferred_element_type=jnp.float32
    ).astype(jnp.bfloat16)


def shards(
    mixer_input,
    decay_shift,
    pole_real,
    pole_imaginary,
    log_step,
    input_map,
    readout_matrix,
    skip,
    out_proj,
    stream,
    norm_gain,
    routes,
    route_logits,
    w_gate,
    w_up,
    w_down,
):
    factors = discretize(pole_real, pole_imaginary, log_step, input_map)
    shares = lax.axis_size("tp")
    own_rows = stream.shape[0]
    activated = mixer(mixer_input, decay_shift, factors, readout_matrix, skip)
    whole_proj = lax.all_gather(out_proj, "tp", axis=0, tiled=True)
    received = exchange(activated.reshape(shares, own_rows, -1), "tp", 1)
    own_activated = jnp.swapaxes(received, 0, 1).reshape(own_rows, -1)
    projected = jnp.dot(own_activated, whole_proj, preferred_element_type=jnp.float32)
    mixed = (stream.astype(jnp.float32) + projected).astype(jnp.bfloat16)
    mixed_wide = mixed.astype(jnp.float32)
    normed = (
        mixed_wide
        * lax.rsqrt(jnp.mean(mixed_wide * mixed_wide, axis=-1, keepdims=True) + EPS)
        * norm_gain
    ).astype(jnp.bfloat16)
    weights = jax.nn.sigmoid(
        jnp.stack(
            [route_logits[:, 0] - route_logits[:, 1], route_logits[:, 1] - route_logits[:, 0]],
            axis=1,
        )
    )
    experts = lax.axis_size("sp") * w_gate.shape[0]
    capacity = 4 * own_rows // experts
    slot_width = experts * capacity
    model = stream.shape[1]
    own_slots = slot_numbers(routes, experts, capacity)
    outgoing = dispatch_rows(own_slots, normed, slot_width)
    arrived = exchange(outgoing.reshape(experts, capacity, model), "sp", 2)
    expert_rows = lax.all_gather(arrived.reshape(-1, model), "tp", axis=0, tiled=True)
    gate = jnp.dot(expert_rows, w_gate[0], preferred_element_type=jnp.float32)
    upward = jnp.dot(expert_rows, w_up[0], preferred_element_type=jnp.float32)
    hidden = (jax.nn.silu(gate) * upward).astype(jnp.bfloat16)
    summed = lax.psum_scatter(
        jnp.dot(hidden, w_down[0], preferred_element_type=jnp.float32).astype(jnp.bfloat16),
        "tp",
        scatter_dimension=0,
        tiled=True,
    )
    expert_out = summed.reshape(-1, capacity, model)
    returned_result = exchange(expert_out, "sp", 3).reshape(slot_width, model)
    picked = (
        jnp.take(returned_result, own_slots, axis=0)
        .astype(jnp.float32)
        .reshape(own_rows, -1, model)
    )
    combined = mixed_wide + jnp.sum(picked * weights[:, :, None], axis=1)
    return combined.astype(jnp.bfloat16)


def solution(mesh):
    return jax.shard_map(
        shards,
        mesh=mesh,
        in_specs=(
            P("sp", "tp"),
            P("sp", "tp"),
            P("tp", None),
            P("tp", None),
            P("tp"),
            P(None, "tp", None, None),
            P(None, "tp", None, None),
            P("tp"),
            P("tp", None),
            P(("sp", "tp"), None),
            P(),
            P(("sp", "tp"), None),
            P(("sp", "tp"), None),
            P("sp", None, "tp"),
            P("sp", None, "tp"),
            P("sp", "tp", None),
        ),
        out_specs=P(("sp", "tp"), None),
        check_vma=False,
    )
```

time: 525 us -> 249 us (0.47)
  blocking collectives: 155 us -> 0 us
  local copies, waits for them, and re-layouts: 95.6 us -> 12.6 us
  Pallas kernels: 0 us -> 77.7 us
  other arithmetic: 64.7 us -> 10.6 us
  waiting for transfers between devices: 133 us -> 85.7 us
  matrix products: 51.8 us -> 44 us
  starting transfers between devices: 5.82 us -> 0.26 us
    all_gather x4 -> x0, blocking collectives: 124 us -> none  [prefix(): pieces = jax.tree.map(lambda part: lax.all_gather(part, axis), value)]
    pallas_call x0 -> x6, Pallas kernels: none -> 77.7 us  [the longest x4 66.1 us: exchange(): pl.pallas_call(functools.partial(exchange_kernel, axis, gather), out_shap...]
    reduce_scatter x1 -> x0, waiting for transfers between devices: 31.1 us -> none  [shards(): lax.psum_scatter(jnp.dot(activated, out_proj, preferred_element_type=jnp....]
    all_to_all x1 -> x0, blocking collectives: 31 us -> none  [shards(): lax.all_to_all(outgoing.reshape(experts, capacity, model), 'sp', split_ax...]
    slice x49 -> x4, local copies, waits for them, and re-layouts: 32 us -> 1.13 us  [the longest x2 1.07 us: discretize(): input_map[1]]
    dynamic_update_slice x16 -> x0, other arithmetic: 25.9 us -> none  [block_states(): lax.scan(advance, (first, empty, empty, empty), (arrange(trans_real), arr...]
    all_to_all x1 -> x0, waiting for transfers between devices: 25.1 us -> none  [shards(): lax.all_to_all(expert_out, 'sp', split_axis=0, concat_axis=0, tiled=True)]
    dynamic_slice x32 -> x0, local copies, waits for them, and re-layouts: 22.5 us -> none  [block_states(): lax.scan(advance, (first, empty, empty, empty), (arrange(trans_real), arr...]
  transfers between devices with their start and end apart: 4 -> 3, of which waited for: 4 -> 2; matrix products, arithmetic and copies ran while one was open for 0% -> 7% of each run, Pallas kernels for 0% -> 12%
where the time goes in v1:
time: 249 us; the launch traced here: 244 us
  waiting for transfers between devices  85.7 us (34%)
  Pallas kernels  77.7 us (31%)
  matrix products  44 us (18%)
  between operations  13.5 us (5%)
  local copies, waits for them, and re-layouts  12.6 us (5%)
  other arithmetic  10.6 us (4%)
    pallas_call x4, Pallas kernels, exchange(): pl.pallas_call(functools.partial(exchange_kernel, axis, gather), out_shap...  66.1 us
    reduce_scatter x1, waiting for transfers between devices, shards(): lax.psum_scatter(jnp.dot(hidden, w_down[0], preferred_element_type=jnp.fl...  44 us
    all_gather x1, waiting for transfers between devices, shards(): lax.all_gather(arrived.reshape(-1, model), 'tp', axis=0, tiled=True)  40.9 us
    dot_general x1, matrix products, shards(): jnp.dot(hidden, w_down[0], preferred_element_type=jnp.float32)  25.8 us
    dot_general x1, matrix products, shards(): gate = jnp.dot(expert_rows, w_gate[0], preferred_element_type=jnp.float32)  13.5 us
    pallas_call x1, Pallas kernels, mixer(): pl.pallas_call(functools.partial(respond_kernel, 'sp'), out_shape=jax.Sha...  6.44 us
    pallas_call x1, Pallas kernels, mixer(): pl.pallas_call(totals_kernel, out_shape=(jax.ShapeDtypeStruct((4, LANES,...  5.17 us
  transfers between devices with their start and end apart: 3, of which 2 were waited for; matrix products, arithmetic and copies ran while one was open for 7% of the time, Pallas kernels for 12%

profile of v1, /device:TPU:0, one launch (start us, length us, event | category | flops | bytes accessed | tf_op | source)
XLA Modules:
  0.0 244.3 jit_solution(10290387214367177864)
XLA Ops:
  6.5 0.7 all-gather.3.cloned.1.call-update
  7.3 0.7 exp.17
  8.0 0.8 fusion.18
  9.0 1.0 fusion.29
  10.0 0.1 squeeze.10
  10.2 0.1 squeeze.22
  10.3 0.1 tile.36
  10.4 0.3 copy.58
  10.8 0.1 tile.38
  10.9 0.3 copy.59
  11.5 0.8 copy.55
  12.2 0.7 copy.73
  13.0 0.6 pad_maximum_fusion.2.factor
  13.6 0.9 select_convert_fusion.3
  14.5 0.9 subtract_convert_fusion.3
  15.4 1.6 pad_maximum_fusion.maps
  17.0 5.2 %totals.1 = (f32[4,8,1024]{2,1,0:T(8,128)}, f32[8,1024]{1,0:T(8,128)}) custom-call(bf16[256,256]{1,0:T(8,128)(2,1)} %bitcast.79, f32[256,16]{1,0:T(8,128)} %bitcast.77, f32[2,1024]{1,0:T(2,128)} %pad_maximum_fusion.2.factor, bf16[4,1024,256]{2,1,0:T(8,128)(2,1)} %pad_maximum_fusion.maps), custom_call_target="tpu_custom_call" | custom-call | tf_op jit(solution)/shard_map/totals/pallas_call | solution.py:236
  22.2 12.3 %exchange_0.1.gathered = f32[8,8,1024]{2,1,0:T(8,128)} custom-call(f32[8,1024]{1,0:T(8,128)} %get-tuple-element.8.value), custom_call_target="tpu_custom_call" | custom-call | tf_op jit(solution)/shard_map/exchange_0/pallas_call | solution.py:74
  34.7 0.3 copy.61
  35.2 0.3 copy.63
  35.5 0.2 select_convert_fusion.1
  35.8 0.3 subtract_convert_fusion.1
  36.1 1.6 pad_maximum_fusion.1.reads
  37.7 6.4 %respond.1 = bf16[256,256]{1,0:T(8,128)(2,1)} custom-call(bf16[256,256]{1,0:T(8,128)(2,1)} %bitcast.80, f32[256,16]{1,0:T(8,128)} %bitcast.78, f32[2,1024]{1,0:T(2,128)} %pad_maximum_fusion.2.factor, bf16[4,1024,256]{2,1,0:T(8,128)(2,1)} %pad_maximum_fusion.maps, f32[4,8,1024]{2,1,0:T(8,128)} %get-tuple-element.7.parts, f32[8,8,1024]{2,1,0:T(8,128)} %exchange_0.1.gathered, ...), custom_call_target="tpu_custom_call" | custom-call | tf_op jit(solution)/shard_map/respond/pallas_call | solution.py:248
  44.1 1.6 copy.64
  45.7 5.7 %exchange_1.1 = bf16[4,64,256]{2,1,0:T(8,128)(2,1)} custom-call(bf16[4,64,256]{2,1,0:T(8,128)(2,1)} %bitcast.83), custom_call_target="tpu_custom_call" | custom-call | tf_op jit(solution)/shard_map/exchange_1/pallas_call | solution.py:74
  51.4 0.9 copy.71
  52.4 0.1 reshape.1278
  52.7 0.2 reduce_window_sum.11
  52.8 0.2 select_reduce_fusion
  53.0 0.1 reduce_sum.44
  53.4 3.2 %multiply_reduce_fusion.1 = (f32[64]{0:T(128)S(1)}, f32[64,2048]{1,0:T(8,128)S(1)}) fusion(bf16[64,1024]{1,0:T(8,128)(2,1)S(1)} %bitcast.87, bf16[1024,2048]{1,0:T(8,128)(2,1)} %all-gather.3.cloned.1.call-done, bf16[64,2048]{1,0:T(8,128)(2,1)S(1)} %copy-done.1), kind=kOutput, calls=%fused_computation.29 | convolution fusion | flops 269221824 | bytes 5112064 | tf_op jit(solution)/shard_map/dot_general | solution.py:300
  56.6 1.5 convolution_convert_fusion
  58.1 24.8 %exchange_2.1 = bf16[8,32,2048]{2,1,0:T(8,128)(2,1)} custom-call(bf16[8,32,2048]{2,1,0:T(8,128)(2,1)} %bitcast.72), custom_call_target="tpu_custom_call" | custom-call | tf_op jit(solution)/shard_map/exchange_2/pallas_call | solution.py:74
  82.9 0.2 reduce-scatter.2.cloned.1.call-start
  83.2 40.9 %all-gather.5.cloned.1.call-done = bf16[1024,2048]{1,0:T(8,128)(2,1)} async-done(((bf16[256,2048]{1,0:T(8,128)(2,1)}), bf16[1024,2048]{1,0:T(8,128)(2,1)}) %all-gather.5.cloned.1.call-update) | async-done | bytes 4194320 | tf_op jit(solution)/shard_map/all_gather | solution.py:321
  124.1 13.5 %fusion.4 = f32[1024,1792]{1,0:T(8,128)} fusion(bf16[1024,2048]{1,0:T(8,128)(2,1)} %all-gather.5.cloned.1.call-done, bf16[1,2048,1792]{2,1,0:T(8,128)(2,1)} %param.29), kind=kOutput, calls=%fused_computation.5 | convolution fusion | flops 7516192768 | bytes 18874368 | tf_op jit(solution)/shard_map/dot_general | solution.py:322
  137.6 25.8 %fusion.8 = bf16[1024,2048]{1,0:T(8,128)(2,1)} fusion(bf16[1,1792,2048]{2,1,0:T(8,128)(2,1)} %param.31, f32[1024,1792]{1,0:T(8,128)} %fusion.4, bf16[1024,2048]{1,0:T(8,128)(2,1)} %all-gather.5.cloned.1.call-done, bf16[1,2048,1792]{2,1,0:T(8,128)(2,1)} %param.30), kind=kOutput, calls=%fused_computation.8 | convolution fusion | flops 15045492736 | bytes 30408704 | tf_op jit(solution)/shard_map/dot_general | solution.py:326
  163.6 0.1 mul.178
  163.7 0.1 copy.68
  163.8 0.3 copy-done.6
  164.1 0.1 copy.70
  164.2 44.0 %reduce-scatter.2.cloned.1.call-done = bf16[256,2048]{1,0:T(8,128)(2,1)} async-done(((bf16[1024,2048]{1,0:T(8,128)(2,1)}), bf16[256,2048]{1,0:T(8,128)(2,1)}) %reduce-scatter.2.cloned.1.call-update) | async-done | bytes 1048592 | tf_op jit(solution)/shard_map/reduce_scatter | solution.py:325
  208.2 23.3 %exchange_3.1 = bf16[8,32,2048]{2,1,0:T(8,128)(2,1)} custom-call(bf16[8,32,2048]{2,1,0:T(8,128)(2,1)} %bitcast.81), custom_call_target="tpu_custom_call" | custom-call | tf_op jit(solution)/shard_map/exchange_3/pallas_call | solution.py:74
  231.5 2.8 %gather_fusion = bf16[128,2048]{1,0:T(8,128)(2,1)S(1)} fusion(bf16[256,2048]{1,0:T(8,128)(2,1)} %bitcast.70, s32[1024]{0:T(1024)S(1)} %pad_clamp_fusion), kind=kCustom, calls=%fused_computation | custom fusion | bytes 1049088 | tf_op jit(solution)/shard_map/jit(_take)/gather | solution.py:334
  234.3 0.3 gather.7
  234.7 2.3 multiply_reduce_fusion
  237.0 0.8 add_convert_fusion
  (47 shorter events, 1.5 us)
Async XLA Ops:
  6.5 46.8 %all-gather.3.cloned.1.call-start = ((), (), s32[]{:S(2)}) async-start(), calls=%async_computation.1 | async-start | bytes 5242880 | tf_op jit(solution)/shard_map/all_gather | solution.py:297
  7.3 4.1 %copy-start.3 = (f32[256,16]{0,1:T(8,128)S(1)}, f32[256,16]{0,1:T(8,128)}, u32[]{:S(2)}) copy-start(f32[256,16]{0,1:T(8,128)} %param.17) | copy-start | bytes 49156
  7.3 116.8 %all-gather.5.cloned.1.call-start = ((), (), s32[]{:S(2)}) async-start(), calls=%async_computation.2 | async-start | bytes 5242880 | tf_op jit(solution)/shard_map/all_gather | solution.py:321
  9.0 3.3 %copy-start.2 = (bf16[256,256]{1,0:T(8,128)(2,1)S(1)}, bf16[256,256]{1,0:T(8,128)(2,1)}, u32[]{:S(2)}) copy-start(bf16[256,256]{1,0:T(8,128)(2,1)} %param.16) | copy-start | bytes 393220
  15.4 19.0 %copy-start = (f32[2,16,16,64]{3,2,1,0:T(8,128)S(1)}, f32[2,16,16,64]{3,2,1,0:T(8,128)}, u32[]{:S(2)}) copy-start(f32[2,16,16,64]{3,2,1,0:T(8,128)} %param.22) | copy-start | bytes 393220
  36.1 16.3 %copy-start.4 = (s32[64,2]{0,1:T(2,128)S(1)}, s32[64,2]{0,1:T(2,128)}, u32[]{:S(2)}) copy-start(s32[64,2]{0,1:T(2,128)} %param.27) | copy-start | bytes 1540
  36.1 17.3 %copy-start.1 = (bf16[64,2048]{1,0:T(8,128)(2,1)S(1)}, bf16[64,2048]{1,0:T(8,128)(2,1)}, u32[]{:S(2)}) copy-start(bf16[64,2048]{1,0:T(8,128)(2,1)} %param.25) | copy-start | bytes 786436
  44.1 12.4 %copy-start.5 = (f32[2048]{0:T(1024)S(1)}, f32[2048]{0:T(1024)}, u32[]{:S(2)}) copy-start(f32[2048]{0:T(1024)} %param.26) | copy-start | bytes 24580
  82.9 125.3 %reduce-scatter.2.cloned.1.call-start = ((), (), s32[]{:S(2)}) async-start(), calls=%async_computation.3 | async-start | bytes 5242880 | tf_op jit(solution)/shard_map/reduce_scatter | solution.py:325
  163.4 0.7 copy-start.6
Sparse Core Ops, SparseCore 0:
  8.9 37.1 all-gather.2
  83.1 40.9 all-gather.4
  163.6 44.6 reduce-scatter.1
